TPU v7x, 32 devices: a whole 2x2x4 slice. The times are simulated.
32 devices in a mesh: ep: 4 (over y, x), tp: 8 (over z, core).
Axes of the slice: x: 2, y: 2, z: 4, core: 2. Of those that a mesh axis runs over, the one named last changes fastest.
Arguments:
- q_latent: bfloat16 [4096, 512], P('ep'), may hold values from -6 to 6
- kv_latent: bfloat16 [4096, 256], P('ep'), may hold values from -6 to 6
- rope_key: bfloat16 [4096, 32], P('ep'), may hold values from -1200 to 1200
- q_gain: float32 [512], replicated, may hold values from 0.1 to 1.9
- kv_gain: float32 [256], replicated, may hold values from 0.1 to 1.9
- w_query: bfloat16 [512, 1536], P(None, 'tp'), may hold values from -0.25 to 0.25
- w_keyval: bfloat16 [256, 2048], P(None, 'tp'), may hold values from -0.375 to 0.375
- w_output: bfloat16 [1024, 2048], P(None, 'tp'), may hold values from -0.1875 to 0.1875
- moe_input: bfloat16 [1024, 2048], P('ep'), may hold values from -6 to 6
- moe_gain: float32 [2048], replicated, may hold values from 0.1 to 1.9
- routes: int32 [1024, 2], P('ep'), may hold values from 0 to 3, all different within a row; in each aligned block of 32 rows (0 to 31, 32 to 63, ...) at most 24 rows name the same one
- route_weight: float32 [1024, 2], P('ep'), may hold values from 0.25 to 2
- expert_gate: bfloat16 [4, 2048, 4096], P('ep', None, 'tp'), may hold values from -0.125 to 0.125
- expert_up: bfloat16 [4, 2048, 4096], P('ep', None, 'tp'), may hold values from -0.125 to 0.125
- expert_down: bfloat16 [4, 4096, 2048], P('ep', 'tp'), may hold values from -0.09375 to 0.09375
- shared_gate: bfloat16 [2048, 2048], P(None, 'tp'), may hold values from -0.125 to 0.125
- shared_up: bfloat16 [2048, 2048], P(None, 'tp'), may hold values from -0.125 to 0.125
- shared_down: bfloat16 [2048, 2048], P('tp'), may hold values from -0.125 to 0.125
Outputs:
- mixed: bfloat16 [4096, 2048], P('ep', 'tp')
- moe_out: bfloat16 [1024, 2048], P(('ep', 'tp'))
Inputs may be any that keep to these rules, and one draw needn't show every extreme that they name: `routes`: in each aligned block of 32 rows (the rows of one device's output) no expert is named by more than 24 rows, a bound that some block reaches. Each row names 2 different experts.
All inputs are finite; a program needn't handle non-finite values.
Results may differ from a plain program's by a relative error of at most 0.023.
Values may be sent and summed in bfloat16 or wider, within the bound.
A program may use at most 128 MiB of HBM per device.

v0:
```python
import jax
import jax.numpy as jnp
from jax import lax
from jax.sharding import PartitionSpec as P

NOPE = 64
ROPE_DIM = 32
VDIM = 64
MOE_DEV = 32
norm_eps = 1e-06
layer_eps = 1e-05
rotary_base = 10000.0
floor_value = -1e30


def rms_scale(values, gain):
    widened = values.astype(jnp.float32)
    return (
        widened * lax.rsqrt(jnp.mean(widened * widened, -1, keepdims=True) + norm_eps) * gain
    ).astype(jnp.bfloat16)


def layer_scale(values, gain):
    widened = values.astype(jnp.float32)
    centred = widened - jnp.mean(widened, -1, keepdims=True)
    return (
        centred * lax.rsqrt(jnp.mean(centred * centred, -1, keepdims=True) + layer_eps) * gain
    ).astype(jnp.bfloat16)


def rotary_tables(positions):
    halfway = ROPE_DIM // 2
    inverse = rotary_base ** (-(jnp.arange(halfway, dtype=jnp.float32) * 2.0 / ROPE_DIM))
    angles = positions.astype(jnp.float32)[:, None] * inverse[None, :]
    return (jnp.cos(angles), jnp.sin(angles))


def rotate(values, cosine_table, sine_table):
    halfway = values.shape[-1] // 2
    first_half = values[..., :halfway]
    second_half = values[..., halfway:]
    return jnp.concatenate(
        [
            first_half * cosine_table - second_half * sine_table,
            second_half * cosine_table + first_half * sine_table,
        ],
        -1,
    )


def block_stats(query_block, query_pos, keyvals, rotated_keys, key_pos):
    scale = float(NOPE + ROPE_DIM) ** (-0.5)
    scores = jnp.einsum(
        "qhd,khd->hqk",
        query_block[..., :NOPE],
        keyvals[..., :NOPE],
        preferred_element_type=jnp.float32,
    )
    scores = (
        scores
        + jnp.einsum(
            "qhd,kd->hqk", query_block[..., NOPE:], rotated_keys, preferred_element_type=jnp.float32
        )
    ) * scale
    allowed = key_pos[None, :] <= query_pos[:, None]
    scores = jnp.where(allowed[None], scores, -jnp.inf)
    block_max = jnp.max(scores, -1)
    weights = jnp.exp(scores - block_max[..., None])
    block_sum = jnp.sum(weights, -1)
    attended = jnp.einsum(
        "hqk,khd->qhd",
        weights.astype(jnp.bfloat16),
        keyvals[..., NOPE:],
        preferred_element_type=jnp.float32,
    ).astype(jnp.bfloat16)
    return (block_max.T, block_sum.T, attended)


def merge_block(carried, stats):
    running_max, running_sum, running_acc = carried
    block_max, block_sum, attended = stats
    new_max = jnp.maximum(running_max, block_max)
    old_weight = jnp.exp(running_max - new_max)
    new_weight = jnp.exp(block_max - new_max)
    return (
        new_max,
        running_sum * old_weight + block_sum * new_weight,
        running_acc * old_weight[..., None] + attended.astype(jnp.float32) * new_weight[..., None],
    )


def body(
    q_latent,
    kv_latent,
    rope_key,
    q_gain,
    kv_gain,
    w_query,
    w_keyval,
    w_output,
    moe_input,
    moe_gain,
    routes,
    route_weight,
    expert_gate,
    expert_up,
    expert_down,
    shared_gate,
    shared_up,
    shared_down,
):
    row_count = q_latent.shape[0]
    own_index = lax.axis_index("ep")
    ep_count = lax.axis_size("ep")
    tp_count = lax.axis_size("tp")
    positions = own_index * row_count + jnp.arange(row_count, dtype=jnp.int32)
    cosine_table, sine_table = rotary_tables(positions)
    q_normed = rms_scale(q_latent, q_gain)
    kv_normed = rms_scale(kv_latent, kv_gain)
    key_rotated = rotate(rope_key.astype(jnp.float32), cosine_table, sine_table).astype(
        jnp.bfloat16
    )
    heads_local = w_query.shape[1] // (NOPE + ROPE_DIM)
    projected = jnp.dot(q_normed, w_query, preferred_element_type=jnp.float32)
    projected = projected.reshape(row_count, heads_local, NOPE + ROPE_DIM)
    queries = jnp.concatenate(
        [
            projected[..., :NOPE],
            rotate(projected[..., NOPE:], cosine_table[:, None, :], sine_table[:, None, :]),
        ],
        -1,
    ).astype(jnp.bfloat16)

    def expand_keys(latent_rows):
        expanded = jnp.dot(latent_rows, w_keyval, preferred_element_type=jnp.float32).astype(
            jnp.bfloat16
        )
        return expanded.reshape(latent_rows.shape[0], heads_local, NOPE + VDIM)

    initial = (
        jnp.full((row_count, heads_local), floor_value, jnp.float32),
        jnp.zeros((row_count, heads_local), jnp.float32),
        jnp.zeros((row_count, heads_local, VDIM), jnp.float32),
    )
    carried = initial
    latent_piece = lax.all_gather(kv_normed, "ep", axis=0, tiled=True)
    rotated_piece = lax.all_gather(key_rotated, "ep", axis=0, tiled=True)
    block_count = latent_piece.shape[0] // row_count

    def visit_block(inner, offset):

        def live(current):
            latent_rows = lax.dynamic_slice_in_dim(latent_piece, offset * row_count, row_count, 0)
            rotated_rows = lax.dynamic_slice_in_dim(rotated_piece, offset * row_count, row_count, 0)
            key_pos = offset * row_count + jnp.arange(row_count, dtype=jnp.int32)
            stats = block_stats(queries, positions, expand_keys(latent_rows), rotated_rows, key_pos)
            return merge_block(current, stats)

        def skipped(current):
            return current

        return (lax.cond(offset <= own_index, live, skipped, inner), None)

    carried, unused = lax.scan(visit_block, carried, jnp.arange(block_count, dtype=jnp.int32))
    running_max, running_sum, running_acc = carried
    heads_out = (
        (running_acc / running_sum[..., None])
        .astype(jnp.bfloat16)
        .reshape(row_count, heads_local * VDIM)
    )
    mixed = jnp.dot(
        lax.all_gather(heads_out, "tp", axis=1, tiled=True),
        w_output,
        preferred_element_type=jnp.float32,
    )
    mixed = mixed.astype(jnp.bfloat16)
    width = moe_input.shape[1]
    top_count = routes.shape[1]
    local_experts = expert_gate.shape[0]
    expert_count = local_experts * ep_count
    capacity = max(2, 3 * MOE_DEV * top_count // (2 * expert_count))
    normed = layer_scale(moe_input, moe_gain)
    entries = routes.reshape(tp_count, MOE_DEV * top_count)
    onehot = (entries[..., None] == jnp.arange(expert_count, dtype=jnp.int32)).astype(jnp.int32)
    earlier = jnp.cumsum(onehot, 1) - onehot
    rank_in = jnp.sum(earlier * onehot, -1)
    block_ids = jnp.arange(tp_count, dtype=jnp.int32)[:, None]
    slot_of = ((entries * tp_count + block_ids) * capacity + rank_in).reshape(-1, top_count)
    token_ids = jnp.arange(tp_count * MOE_DEV * top_count, dtype=jnp.int32) // top_count
    slot_token = (
        jnp.full((expert_count * tp_count * capacity,), -1, jnp.int32)
        .at[slot_of.reshape(-1)]
        .set(token_ids)
    )
    outgoing = jnp.where(
        (slot_token >= 0)[:, None], normed[jnp.maximum(slot_token, 0)], jnp.zeros((), jnp.bfloat16)
    )
    outgoing = outgoing.reshape(ep_count, local_experts, tp_count, capacity, width)
    arrived = lax.all_to_all(outgoing, "ep", split_axis=0, concat_axis=0, tiled=True)
    slot_rows = arrived.shape[3]
    inputs = arrived[:, 0].reshape(-1, width)
    hidden = jax.nn.silu(jnp.dot(inputs, expert_gate[0], preferred_element_type=jnp.float32))
    hidden = (hidden * jnp.dot(inputs, expert_up[0], preferred_element_type=jnp.float32)).astype(
        jnp.bfloat16
    )
    output = jnp.dot(hidden, expert_down[0], preferred_element_type=jnp.float32)
    results = [output.astype(jnp.bfloat16).reshape(ep_count, tp_count, slot_rows, width)]
    partial_value = jnp.stack(results, 1)
    shared_hidden = jax.nn.silu(jnp.dot(normed, shared_gate, preferred_element_type=jnp.float32))
    shared_hidden = (
        shared_hidden * jnp.dot(normed, shared_up, preferred_element_type=jnp.float32)
    ).astype(jnp.bfloat16)
    shared_part = jnp.dot(shared_hidden, shared_down, preferred_element_type=jnp.float32).astype(
        jnp.bfloat16
    )
    slot_total, shared_total = (
        lax.psum_scatter(
            partial_value.astype(jnp.float32).astype(jnp.bfloat16),
            "tp",
            scatter_dimension=2,
            tiled=True,
        ).astype(jnp.float32),
        lax.psum_scatter(
            shared_part.astype(jnp.float32)
            .reshape(1, 1, tp_count, MOE_DEV, width)
            .astype(jnp.bfloat16),
            "tp",
            scatter_dimension=2,
            tiled=True,
        ).astype(jnp.float32),
    )
    arrived_sums = lax.all_to_all(
        slot_total.astype(jnp.bfloat16), "ep", split_axis=0, concat_axis=0, tiled=True
    ).astype(slot_total.dtype)
    own_block = lax.axis_index("tp")
    own_entries = lax.dynamic_slice_in_dim(routes, own_block * MOE_DEV, MOE_DEV, 0)
    own_rank = lax.dynamic_slice_in_dim(
        rank_in.reshape(-1, top_count), own_block * MOE_DEV, MOE_DEV, 0
    )
    own_weight = lax.dynamic_slice_in_dim(route_weight, own_block * MOE_DEV, MOE_DEV, 0)
    picked = arrived_sums.reshape(-1, width)[own_entries * capacity + own_rank]
    moe_out = (
        jnp.sum(own_weight[..., None] * picked, 1) + shared_total.reshape(MOE_DEV, width)
    ).astype(jnp.bfloat16)
    return (mixed, moe_out)


def solution(mesh):
    in_specs = (
        P("ep", None),
        P("ep", None),
        P("ep", None),
        P(),
        P(),
        P(None, "tp"),
        P(None, "tp"),
        P(None, "tp"),
        P("ep", None),
        P(),
        P("ep", None),
        P("ep", None),
        P("ep", None, "tp"),
        P("ep", None, "tp"),
        P("ep", "tp", None),
        P(None, "tp"),
        P(None, "tp"),
        P("tp", None),
    )
    out_specs = (P("ep", "tp"), P(("ep", "tp"), None))
    return jax.shard_map(body, mesh=mesh, in_specs=in_specs, out_specs=out_specs, check_vma=False)
```

profile of v0, /device:TPU:0, one launch (start us, length us, event | category | flops | bytes accessed | tf_op | source)
XLA Modules:
  0.0 239.6 jit_solution(11745356198436479961)
XLA Ops:
  8.0 1.0 copy.32
  9.0 0.7 broadcast_multiply_fusion
  9.9 1.4 fusion.80
  11.8 2.4 %scatter_custom_fusion = s32[768]{0:T(1024)S(1)} fusion(s32[512]{0:T(512)S(1)} %bitcast.88, s32[512]{0:T(512)S(1)} %add_select_fusion, s32[]{:T(128)} %constant.90.clone.1), kind=kCustom, calls=%fused_computation.110 | custom fusion | bytes 3076 | tf_op jit(solution)/shard_map/scatter | solution.py:193
  14.3 1.4 convert_reduce_fusion
  16.3 1.6 fusion.40
  17.9 4.3 %gather_fusion = bf16[768,2048]{1,0:T(8,128)(2,1)} fusion(bf16[256,2048]{1,0:T(8,128)(2,1)S(1)} %fusion.40, s32[1024]{0:T(1024)S(1)} %pad_clamp_fusion.1), kind=kCustom, calls=%fused_computation | custom fusion | bytes 6294528 | tf_op jit(solution)/shard_map/gather | solution.py:196
  22.2 3.8 %broadcast_select_fusion = bf16[4,1,8,24,2048]{4,3,2,1,0:T(8,128)(2,1)} fusion(bf16[4,1,8,24,2048]{4,3,2,1,0:T(8,128)(2,1)} %bitcast.82, pred[4,8,24]{2,1,0:T(8,128)(4,1)S(1)} %broadcast_in_dim.44), kind=kLoop, calls=%fused_computation.38 | loop fusion | flops 1572864 | bytes 6292224 | tf_op jit(solution)/shard_map/jit(_where)/select_n | solution.py:195
  26.0 5.3 %all-to-all-start = ((bf16[4,1,8,24,2048]{4,3,2,1,0:T(8,128)(2,1)}), bf16[4,1,8,24,2048]{4,3,2,1,0:T(8,128)(2,1)}, u32[]{:S(2)}, u32[]{:S(2)}) async-start(bf16[4,1,8,24,2048]{4,3,2,1,0:T(8,128)(2,1)} %broadcast_select_fusion), calls=%async_computation | async-start | bytes 6291456 | tf_op jit(solution)/shard_map/all_to_all | solution.py:199
  31.4 1.3 fusion.52
  32.6 2.0 fusion.54
  34.8 39.4 %all-to-all-done = bf16[4,1,8,24,2048]{4,3,2,1,0:T(8,128)(2,1)} async-done(((bf16[4,1,8,24,2048]{4,3,2,1,0:T(8,128)(2,1)}), bf16[4,1,8,24,2048]{4,3,2,1,0:T(8,128)(2,1)}, u32[]{:S(2)}, u32[]{:S(2)}) %all-to-all-start) | async-done | bytes 3145760 | tf_op jit(solution)/shard_map/all_to_all | solution.py:199
  74.1 5.6 %fusion.47 = f32[768,512]{1,0:T(8,128)} fusion(bf16[768,2048]{1,0:T(8,128)(2,1)} %bitcast.12, bf16[1,2048,512]{2,1,0:T(8,128)(2,1)} %param.34), kind=kOutput, calls=%fused_computation.55 | convolution fusion | flops 1610612736 | bytes 6815744 | tf_op jit(solution)/shard_map/dot_general | solution.py:202
  79.7 8.2 %convolution_convert_fusion.1 = bf16[768,2048]{1,0:T(8,128)(2,1)} fusion(bf16[1,512,2048]{2,1,0:T(8,128)(2,1)S(1)} %copy-done, f32[768,512]{1,0:T(8,128)} %fusion.47, bf16[768,2048]{1,0:T(8,128)(2,1)} %bitcast.12, bf16[1,2048,512]{2,1,0:T(8,128)(2,1)} %param.35), kind=kOutput, calls=%fused_computation.37 | convolution fusion | flops 3225157632 | bytes 12058624 | tf_op jit(solution)/shard_map/dot_general | solution.py:206
  88.0 1.7 fusion.81
  89.7 3.9 %convolution_convert_fusion.2 = bf16[256,2048]{1,0:T(8,128)(2,1)} fusion(bf16[256,2048]{1,0:T(8,128)(2,1)} %param.39, bf16[256,2048]{1,0:T(8,128)(2,1)S(1)} %fusion.40, bf16[2048,256]{1,0:T(8,128)(2,1)} %param.38, f32[256,256]{1,0:T(8,128)S(1)} %fusion.81), kind=kOutput, calls=%fused_computation.43 | convolution fusion | flops 537788416 | bytes 4456448 | tf_op jit(solution)/shard_map/dot_general | solution.py:213
  93.7 0.9 convert_element_type.97
  94.6 1.5 fusion.41
  96.1 1.5 fusion.55
  97.7 0.9 copy-done.4
  99.0 9.5 %all_gather.10 = bf16[4096,32]{0,1:T(8,128)(2,1)S(1)} all-gather(bf16[1024,32]{0,1:T(8,128)(2,1)S(1)} %pad_maximum_fusion.1), channel_id=1, replica_groups=mesh['ep'=4,'tp'=8] {'ep'}, dimensions={0}, use_global_device_ids=true | all-gather | bytes 327680 | tf_op jit(solution)/shard_map/all_gather | solution.py:147
  108.4 1.0 subtract_convert_fusion
  109.5 0.5 iota.29
  110.1 0.6 broadcast_in_dim.40
  110.7 16.7 %while.15 = (s32[]{:T(128)}, f32[1024,2]{0,1:T(2,128)}, f32[1024,2]{0,1:T(2,128)S(1)}, f32[1024,2,64]{0,2,1:T(8,128)S(1)}, s32[4]{0:T(128)}, /*index=5*/s32[]{:T...) while((s32[]{:T(128)}, f32[1024,2]{0,1:T(2,128)}, ...), condition=%wide.region_7.8_spmd.clone, body=%wide.region_2.7_spmd.clone.sunk | while | flops 824059904 | bytes 47456656 | solution.py:164
  110.7 1.3 dynamic_slice.35
  112.6 8.7 %conditional.3 = ((f32[1024,2]{0,1:T(2,128)}, f32[1024,2]{0,1:T(2,128)S(1)}, f32[1024,2,64]{0,2,1:T(8,128)S(1)})) conditional(s32[]{:T(128)} %convert_element_type.190, (f32[1024,2]{0,1:T(2,128)}, f32[1024,2]{0,1:T(2,128)S(1)}, f32[1024,2,64]{0,2,1:T(8,128)S(1)}) %tuple.45, (s32[]{:T(128)}, s32[]{:T(128)}, bf16[4096,256]{1,0:T(8,128)(2,1)}, ...), branch_computations={%region_3.3_spmd, %region_4.6_spmd} | conditional | flops 824059904 | bytes 47452312 | solution.py:162
  113.3 1.4 convolution_convert_fusion
  114.7 1.3 fusion.26
  116.0 0.7 broadcast_compare_fusion
  116.7 2.0 fusion.79
  118.7 1.1 fusion.5
  119.9 1.5 fusion.21
  121.4 1.3 dynamic_slice.35
  123.4 1.3 dynamic_slice.35
  125.4 1.3 dynamic_slice.35
  127.4 0.8 divide_convert_fusion
  128.3 1.2 dynamic-slice
  129.6 35.7 %all-reduce.3.cloned.1.call-done = bf16[4,1,8,24,2048]{4,3,2,0,1:T(8,128)(2,1)} async-done(((bf16[4,1,8,24,2048]{4,3,2,0,1:T(8,128)(2,1)}), bf16[4,1,8,24,2048]{4,3,2,0,1:T(8,128)(2,1)}) %all-reduce.3.cloned.1.call-update) | async-done | bytes 3145744
  165.3 2.4 %dynamic-slice_bitcast_fusion = bf16[4,1,1,24,2048]{4,3,2,1,0:T(8,128)(2,1)} fusion(bf16[4,1,8,24,2048]{4,3,2,0,1:T(8,128)(2,1)} %all-reduce.3.cloned.1.call-done, u32[]{:T(128)} %bitcast.27), kind=kLoop, calls=%fused_computation.76 | loop fusion | bytes 786436 | tf_op jit(solution)/shard_map/reduce_scatter | solution.py:217
  167.7 3.6 %all-to-all-start.1 = ((bf16[4,1,1,24,2048]{4,3,2,1,0:T(8,128)(2,1)}), bf16[4,1,1,24,2048]{4,3,2,1,0:T(8,128)(2,1)S(1)}, u32[]{:S(2)}, u32[]{:S(2)}) async-start(bf16[4,1,1,24,2048]{4,3,2,1,0:T(8,128)(2,1)} %dynamic-slice_bitcast_fusion), calls=%async_computation.1 | async-start | bytes 786432 | tf_op jit(solution)/shard_map/all_to_all | solution.py:232
  171.6 5.6 %all-to-all-done.1 = bf16[4,1,1,24,2048]{4,3,2,1,0:T(8,128)(2,1)S(1)} async-done(((bf16[4,1,1,24,2048]{4,3,2,1,0:T(8,128)(2,1)}), bf16[4,1,1,24,2048]{4,3,2,1,0:T(8,128)(2,1)S(1)}, u32[]{:S(2)}, u32[]{:S(2)}) %all-to-all-start.1) | async-done | bytes 393248 | tf_op jit(solution)/shard_map/all_to_all | solution.py:232
  177.3 0.8 gather_fusion.1
  178.4 0.7 multiply_reduce_fusion
  179.1 20.7 %reduce-scatter.3.cloned.1.call-done = bf16[1,1,1,32,2048]{4,3,2,1,0:T(8,128)(2,1)} async-done(((bf16[1,1,8,32,2048]{4,3,2,1,0:T(8,128)(2,1)}), bf16[1,1,1,32,2048]{4,3,2,1,0:T(8,128)(2,1)}) %reduce-scatter.3.cloned.1.call-update) | async-done | bytes 131088 | tf_op jit(solution)/shard_map/reduce_scatter | solution.py:223
  199.9 1.6 fusion.62
  201.4 27.3 %all-gather.5.cloned.1.call-done = bf16[1024,1024]{0,1:T(8,128)(2,1)} async-done(((bf16[1024,128]{0,1:T(8,128)(2,1)}), bf16[1024,1024]{0,1:T(8,128)(2,1)}) %all-gather.5.cloned.1.call-update) | async-done | bytes 2097168 | tf_op jit(solution)/shard_map/all_gather | solution.py:172
  228.8 3.2 %convolution_convert_fusion.3 = bf16[1024,256]{1,0:T(8,128)(2,1)} fusion(bf16[1024,1024]{0,1:T(8,128)(2,1)} %all-gather.5.cloned.1.call-done, bf16[1024,256]{1,0:T(8,128)(2,1)} %param.29), kind=kOutput, calls=%fused_computation.60 | convolution fusion | flops 537133056 | bytes 3145728 | tf_op jit(solution)/shard_map/dot_general | solution.py:171
  (74 shorter events, 2.9 us)
Async XLA Ops:
  8.0 71.7 %copy-start = (bf16[1,512,2048]{2,1,0:T(8,128)(2,1)S(1)}, bf16[1,512,2048]{2,1,0:T(8,128)(2,1)}, u32[]{:S(2)}) copy-start(bf16[1,512,2048]{2,1,0:T(8,128)(2,1)} %param.36) | copy-start | bytes 6291460
  8.0 7.7 %copy-start.1 = (bf16[256,2048]{1,0:T(8,128)(2,1)S(1)}, bf16[256,2048]{1,0:T(8,128)(2,1)}, u32[]{:S(2)}) copy-start(bf16[256,2048]{1,0:T(8,128)(2,1)} %param.30) | copy-start | bytes 3145732
  8.0 8.3 %copy-start.7 = (f32[2048]{0:T(1024)S(1)}, f32[2048]{0:T(1024)}, u32[]{:S(2)}) copy-start(f32[2048]{0:T(1024)} %param.31) | copy-start | bytes 24580
  26.0 6.6 %copy-start.8 = (f32[256]{0:T(256)S(1)}, f32[256]{0:T(256)}, u32[]{:S(2)}) copy-start(f32[256]{0:T(256)} %param.26) | copy-start | bytes 3076
  26.0 48.1 %all-to-all-start = ((bf16[4,1,8,24,2048]{4,3,2,1,0:T(8,128)(2,1)}), bf16[4,1,8,24,2048]{4,3,2,1,0:T(8,128)(2,1)}, u32[]{:S(2)}, u32[]{:S(2)}) async-start(bf16[4,1,8,24,2048]{4,3,2,1,0:T(8,128)(2,1)} %broadcast_select_fusion), calls=%async_computation | async-start | bytes 6291456 | tf_op jit(solution)/shard_map/all_to_all | solution.py:199
  31.4 78.1 %all-gather.3.cloned.1.call-start = ((), (), s32[]{:S(2)}) async-start(), calls=%async_computation.3 | async-start | bytes 2621440 | tf_op jit(solution)/shard_map/all_gather | solution.py:146
  34.7 130.6 %all-reduce.3.cloned.1.call-start = ((), (), s32[]{:S(2)}) async-start(), calls=%async_computation.6 | async-start | bytes 6291456
  88.0 111.9 %reduce-scatter.3.cloned.1.call-start = ((), (), s32[]{:S(2)}) async-start(), calls=%async_computation.5 | async-start | bytes 1179648 | tf_op jit(solution)/shard_map/reduce_scatter | solution.py:223
  93.6 2.5 %copy-start.3 = (bf16[1024,512]{1,0:T(8,128)(2,1)S(1)}, bf16[1024,512]{1,0:T(8,128)(2,1)}, u32[]{:S(2)}) copy-start(bf16[1024,512]{1,0:T(8,128)(2,1)} %param.22) | copy-start | bytes 3145732
  93.6 2.5 %copy-start.10 = (f32[512]{0:T(512)S(1)}, f32[512]{0:T(512)}, u32[]{:S(2)}) copy-start(f32[512]{0:T(512)} %param.25) | copy-start | bytes 6148
  93.6 135.2 %all-gather.5.cloned.1.call-start = ((), (), s32[]{:S(2)}) async-start(), calls=%async_computation.4 | async-start | bytes 2359296 | tf_op jit(solution)/shard_map/all_gather | solution.py:172
  97.7 0.9 copy-start.4
  97.7 13.0 %copy-start.2 = (bf16[256,256]{1,0:T(8,128)(2,1)S(1)}, bf16[256,256]{1,0:T(8,128)(2,1)}, u32[]{:S(2)}) copy-start(bf16[256,256]{1,0:T(8,128)(2,1)} %param.28) | copy-start | bytes 393220
  118.7 1.1 copy-start.5
  119.8 1.5 copy-start.6
  127.4 44.1 %copy-start.9 = (f32[256,2]{0,1:T(2,128)S(1)}, f32[256,2]{0,1:T(2,128)}, u32[]{:S(2)}) copy-start(f32[256,2]{0,1:T(2,128)} %param.33) | copy-start | bytes 6148
  167.7 9.5 %all-to-all-start.1 = ((bf16[4,1,1,24,2048]{4,3,2,1,0:T(8,128)(2,1)}), bf16[4,1,1,24,2048]{4,3,2,1,0:T(8,128)(2,1)S(1)}, u32[]{:S(2)}, u32[]{:S(2)}) async-start(bf16[4,1,1,24,2048]{4,3,2,1,0:T(8,128)(2,1)} %dynamic-slice_bitcast_fusion), calls=%async_computation.1 | async-start | bytes 786432 | tf_op jit(solution)/shard_map/all_to_all | solution.py:232
Sparse Core Ops, SparseCore 0:
  34.8 58.6 all-gather.2
Sparse Core Ops, SparseCore 1:
  88.0 77.2 all-reduce.2
  167.4 32.4 reduce-scatter.2
  201.3 27.4 all-gather.4
where the time goes:
time: 241 us; the launch traced here: 240 us
  waiting for transfers between devices  129 us (54%)
  matrix products  30.3 us (13%)
  other arithmetic  21.5 us (9%)
  local copies, waits for them, and re-layouts  21 us (9%)
  between operations  16 us (7%)
  blocking collectives  9.47 us (4%)
  starting transfers between devices  9.1 us (4%)
  loops' own time  3.42 us (1%)
    all_to_all x1, waiting for transfers between devices, body(): lax.all_to_all(outgoing, 'ep', split_axis=0, concat_axis=0, tiled=True)  39.4 us
    unnamed x5, waiting for transfers between devices  35.8 us
    all_gather x1, waiting for transfers between devices, body(): lax.all_gather(heads_out, 'tp', axis=1, tiled=True)  27.3 us
    reduce_scatter x1, waiting for transfers between devices, body(): lax.psum_scatter(shared_part.astype(jnp.float32).reshape(1, 1, tp_count,...  20.7 us
    all_gather x1, blocking collectives, body(): rotated_piece = lax.all_gather(key_rotated, 'ep', axis=0, tiled=True)  9.47 us
    dot_general x1, matrix products, body(): output = jnp.dot(hidden, expert_down[0], preferred_element_type=jnp.float32)  8.25 us
    all_to_all x1, waiting for transfers between devices, body(): lax.all_to_all(slot_total.astype(jnp.bfloat16), 'ep', split_axis=0, conca...  5.58 us
    dot_general x1, matrix products, body(): jnp.dot(inputs, expert_gate[0], preferred_element_type=jnp.float32)  5.57 us
  transfers between devices with their start and end apart: 6, of which 5 were waited for; matrix products, arithmetic and copies ran while one was open for 21% of the time, Pallas kernels for 0%

commit v1 on v0

--- a/solution.py
+++ b/solution.py
@@ -168,11 +168,44 @@
         .astype(jnp.bfloat16)
         .reshape(row_count, heads_local * VDIM)
     )
-    mixed = jnp.dot(
-        lax.all_gather(heads_out, "tp", axis=1, tiled=True),
-        w_output,
-        preferred_element_type=jnp.float32,
-    )
+
+    def meet_edges(x_local):
+        all_values, right_arr, o_now = (
+            jax.lax.axis_size("tp"),
+            jax.lax.axis_index("tp"),
+            x_local.shape[1],
+        )
+        frames = []
+        ii = 0
+        while ii < all_values:
+            frames.append((ii, (ii + 1) % all_values))
+            ii += 1
+        windows = []
+        ii = 0
+        while ii < all_values:
+            windows.append((ii, (ii - 1) % all_values))
+            ii += 1
+        w_next = jnp.zeros(
+            (*x_local.shape[:1], all_values * o_now, *x_local.shape[2:]), x_local.dtype
+        )
+        w_next = lax.dynamic_update_slice_in_dim(w_next, x_local, right_arr * o_now, axis=1)
+        new = vec_out = x_local
+        found_now = all_values // 2
+        k0 = 1
+        while k0 < found_now + 1:
+            new = jax.lax.ppermute(new, "tp", frames)
+            w_next = lax.dynamic_update_slice_in_dim(
+                w_next, new, (right_arr - k0) % all_values * o_now, axis=1
+            )
+            if k0 < all_values - found_now:
+                vec_out = jax.lax.ppermute(vec_out, "tp", windows)
+                w_next = lax.dynamic_update_slice_in_dim(
+                    w_next, vec_out, (right_arr + k0) % all_values * o_now, axis=1
+                )
+            k0 = k0 + 1
+        return w_next
+
+    mixed = jnp.dot(meet_edges(heads_out), w_output, preferred_element_type=jnp.float32)
     mixed = mixed.astype(jnp.bfloat16)
     width = moe_input.shape[1]
     top_count = routes.shape[1]

time: 241 us -> 228 us (0.946)
  waiting for transfers between devices: 129 us -> 83.5 us
  starting transfers between devices: 9.1 us -> 28.2 us
  local copies, waits for them, and re-layouts: 21 us -> 31.7 us
    all_gather x1 -> x0, waiting for transfers between devices: 27.3 us -> none  [body(): lax.all_gather(heads_out, 'tp', axis=1, tiled=True)]
    unnamed x5 -> x4, waiting for transfers between devices: 35.8 us -> 14.1 us
    ppermute x0 -> x7, waiting for transfers between devices: none -> 18.5 us  [the longest x3 15.9 us: meet_edges(): vec_out = jax.lax.ppermute(vec_out, 'tp', windows)]
    ppermute x0 -> x7, starting transfers between devices: none -> 11.1 us  [the longest x3 11 us: meet_edges(): vec_out = jax.lax.ppermute(vec_out, 'tp', windows)]
    all_to_all x1, starting transfers between devices: 3.65 us -> 11.7 us  [body(): lax.all_to_all(slot_total.astype(jnp.bfloat16), 'ep', split_axis=0, conca...]
    dynamic_update_slice x0 -> x8, local copies, waits for them, and re-layouts: none -> 6.73 us  [the longest x4 3.85 us: meet_edges(): lax.dynamic_update_slice_in_dim(w_next, new, (right_arr - k0) % all_value...]
    all_to_all x1, waiting for transfers between devices: 39.4 us -> 34.2 us  [body(): lax.all_to_all(outgoing, 'ep', split_axis=0, concat_axis=0, tiled=True)]
    all_to_all x1, waiting for transfers between devices: 5.58 us -> 0.46 us  [body(): lax.all_to_all(slot_total.astype(jnp.bfloat16), 'ep', split_axis=0, conca...]
  transfers between devices with their start and end apart: 6 -> 12, of which waited for: 5 -> 7; matrix products, arithmetic and copies ran while one was open for 21% -> 28% of each run, Pallas kernels for 0% -> 0%
where the time goes in v1:
time: 228 us; the launch traced here: 227 us
  waiting for transfers between devices  83.5 us (37%)
  local copies, waits for them, and re-layouts  31.7 us (14%)
  matrix products  31.2 us (14%)
  starting transfers between devices  28.2 us (12%)
  other arithmetic  22.7 us (10%)
  between operations  16 us (7%)
  blocking collectives  9.97 us (4%)
  loops' own time  3.35 us (1%)
    all_to_all x1, waiting for transfers between devices, body(): lax.all_to_all(outgoing, 'ep', split_axis=0, concat_axis=0, tiled=True)  34.2 us
    reduce_scatter x1, waiting for transfers between devices, body(): lax.psum_scatter(shared_part.astype(jnp.float32).reshape(1, 1, tp_count,...  16.2 us
    ppermute x3, waiting for transfers between devices, meet_edges(): vec_out = jax.lax.ppermute(vec_out, 'tp', windows)  15.9 us
    unnamed x4, waiting for transfers between devices  14.1 us
    all_to_all x1, starting transfers between devices, body(): lax.all_to_all(slot_total.astype(jnp.bfloat16), 'ep', split_axis=0, conca...  11.7 us
    ppermute x3, starting transfers between devices, meet_edges(): vec_out = jax.lax.ppermute(vec_out, 'tp', windows)  11 us
    all_gather x1, blocking collectives, body(): rotated_piece = lax.all_gather(key_rotated, 'ep', axis=0, tiled=True)  9.97 us
    dot_general x1, matrix products, body(): output = jnp.dot(hidden, expert_down[0], preferred_element_type=jnp.float32)  8.24 us
  transfers between devices with their start and end apart: 12, of which 7 were waited for; matrix products, arithmetic and copies ran while one was open for 28% of the time, Pallas kernels for 0%

profile of v1, /device:TPU:0, one launch (start us, length us, event | category | flops | bytes accessed | tf_op | source)
XLA Modules:
  0.0 226.6 jit_solution(6545257784724455926)
XLA Ops:
  8.0 1.0 copy.32
  9.9 1.4 fusion.80
  11.9 2.4 %scatter_custom_fusion = s32[768]{0:T(1024)S(1)} fusion(s32[512]{0:T(512)S(1)} %bitcast.90, s32[512]{0:T(512)S(1)} %add_select_fusion, s32[]{:T(128)} %constant.133.clone.1), kind=kCustom, calls=%fused_computation.119 | custom fusion | bytes 3076 | tf_op jit(solution)/shard_map/scatter | solution.py:226
  14.3 1.4 convert_reduce_fusion
  16.3 1.6 fusion.40
  18.0 4.3 %gather_fusion = bf16[768,2048]{1,0:T(8,128)(2,1)} fusion(bf16[256,2048]{1,0:T(8,128)(2,1)S(1)} %fusion.40, s32[1024]{0:T(1024)S(1)} %pad_clamp_fusion.1), kind=kCustom, calls=%fused_computation | custom fusion | bytes 6294528 | tf_op jit(solution)/shard_map/gather | solution.py:229
  22.3 3.8 %broadcast_select_fusion = bf16[4,1,8,24,2048]{4,3,2,1,0:T(8,128)(2,1)} fusion(bf16[4,1,8,24,2048]{4,3,2,1,0:T(8,128)(2,1)} %bitcast.82, pred[4,8,24]{2,1,0:T(8,128)(4,1)S(1)} %broadcast_in_dim.51), kind=kLoop, calls=%fused_computation.38 | loop fusion | flops 1572864 | bytes 6292224 | tf_op jit(solution)/shard_map/jit(_where)/select_n | solution.py:228
  26.1 5.3 %all-to-all-start = ((bf16[4,1,8,24,2048]{4,3,2,1,0:T(8,128)(2,1)}), bf16[4,1,8,24,2048]{4,3,2,1,0:T(8,128)(2,1)}, u32[]{:S(2)}, u32[]{:S(2)}) async-start(bf16[4,1,8,24,2048]{4,3,2,1,0:T(8,128)(2,1)} %broadcast_select_fusion), calls=%async_computation | async-start | bytes 6291456 | tf_op jit(solution)/shard_map/all_to_all | solution.py:232
  31.4 1.3 fusion.52
  32.8 2.0 fusion.54
  35.0 1.5 fusion.41
  36.5 1.8 fusion.55
  38.3 0.9 copy-done.6
  40.0 34.2 %all-to-all-done = bf16[4,1,8,24,2048]{4,3,2,1,0:T(8,128)(2,1)} async-done(((bf16[4,1,8,24,2048]{4,3,2,1,0:T(8,128)(2,1)}), bf16[4,1,8,24,2048]{4,3,2,1,0:T(8,128)(2,1)}, u32[]{:S(2)}, u32[]{:S(2)}) %all-to-all-start) | async-done | bytes 3145760 | tf_op jit(solution)/shard_map/all_to_all | solution.py:232
  74.2 5.5 %fusion.47 = f32[768,512]{1,0:T(8,128)} fusion(bf16[768,2048]{1,0:T(8,128)(2,1)} %bitcast.12, bf16[1,2048,512]{2,1,0:T(8,128)(2,1)} %param.34), kind=kOutput, calls=%fused_computation.55 | convolution fusion | flops 1610612736 | bytes 6815744 | tf_op jit(solution)/shard_map/dot_general | solution.py:235
  79.7 8.2 %convolution_convert_fusion.1 = bf16[768,2048]{1,0:T(8,128)(2,1)} fusion(bf16[1,512,2048]{2,1,0:T(8,128)(2,1)S(1)} %copy-done, f32[768,512]{1,0:T(8,128)} %fusion.47, bf16[768,2048]{1,0:T(8,128)(2,1)} %bitcast.12, bf16[1,2048,512]{2,1,0:T(8,128)(2,1)} %param.35), kind=kOutput, calls=%fused_computation.37 | convolution fusion | flops 3225157632 | bytes 12058624 | tf_op jit(solution)/shard_map/dot_general | solution.py:239
  88.4 10.0 %all_gather.7 = bf16[4096,32]{0,1:T(8,128)(2,1)} all-gather(bf16[1024,32]{0,1:T(8,128)(2,1)S(1)} %pad_maximum_fusion.1), channel_id=1, replica_groups=mesh['ep'=4,'tp'=8] {'ep'}, dimensions={0}, use_global_device_ids=true | all-gather | bytes 327680 | tf_op jit(solution)/shard_map/all_gather | solution.py:147
  98.3 1.0 subtract_convert_fusion
  99.3 1.0 pad_maximum_fusion
  100.3 1.1 fusion.81
  102.1 0.8 broadcast_in_dim.45
  103.5 18.5 %while.15 = (s32[]{:T(128)}, f32[1024,2]{0,1:T(2,128)}, f32[1024,2]{0,1:T(2,128)S(1)}, f32[1024,2,64]{0,2,1:T(8,128)}, s32[4]{0:T(128)}, /*index=5*/s32[]{:T(128...) while((s32[]{:T(128)}, f32[1024,2]{0,1:T(2,128)}, ...), condition=%wide.region_7.8_spmd.clone, body=%wide.region_2.7_spmd.clone.sunk | while | flops 824059904 | bytes 51651016 | solution.py:164
  103.5 1.3 dynamic_slice.35
  105.5 10.6 %conditional.3 = ((f32[1024,2]{0,1:T(2,128)}, f32[1024,2]{0,1:T(2,128)S(1)}, f32[1024,2,64]{0,2,1:T(8,128)})) conditional(s32[]{:T(128)} %convert_element_type.190, (f32[1024,2]{0,1:T(2,128)}, f32[1024,2]{0,1:T(2,128)S(1)}, f32[1024,2,64]{0,2,1:T(8,128)}) %tuple.45, (s32[]{:T(128)}, s32[]{:T(128)}, bf16[4096,256]{1,0:T(8,128)(2,1)}, ...), branch_computations={%region_3.3_spmd, %region_4.6_spmd} | conditional | flops 824059904 | bytes 51646672 | solution.py:162
  106.1 1.4 convolution_convert_fusion
  107.5 1.3 fusion.26
  109.5 3.0 %fusion.79 = (f32[2,1024]{1,0:T(2,128)S(1)}, f32[2,1024,1024]{1,2,0:T(8,128)S(1)}) fusion(bf16[1024,2,96]{0,2,1:T(8,128)(2,1)S(1)} %get-tuple-element.73, bf16[4096,32]{0,1:T(8,128)(2,1)} %get-tuple-element.74, s32[]{:T(128)S(6)} %select_n.76, f32[2,1024,1024]{2,1,0:T(8,128)S(1)} %fusion.26, pred[1024,1024]{0,1:T(8,128)(4,1)S(1)} %broadcast_compare_fusion), kind=kOutput, calls=%fused_computation.128 | convolution fusion | flops 142604288 | bytes 18030596 | tf_op jit(solution)/shard_map/while/body/eval_jaxpr/cond/branch_1_fun/qhd,kd->hqk/dot_general | solution.py:61
  112.5 1.1 fusion.5
  113.7 1.5 fusion.21
  116.0 1.3 dynamic_slice.35
  118.0 1.3 dynamic_slice.35
  120.0 1.3 dynamic_slice.35
  122.0 1.1 divide_convert_fusion
  123.2 4.0 %convolution_convert_fusion.2 = bf16[256,2048]{1,0:T(8,128)(2,1)} fusion(bf16[256,2048]{1,0:T(8,128)(2,1)} %param.39, bf16[256,2048]{1,0:T(8,128)(2,1)S(1)} %fusion.40, bf16[2048,256]{1,0:T(8,128)(2,1)} %param.38, f32[256,256]{1,0:T(8,128)} %fusion.81), kind=kOutput, calls=%fused_computation.43 | convolution fusion | flops 537788416 | bytes 4456448 | tf_op jit(solution)/shard_map/dot_general | solution.py:246
  127.4 3.6 %collective-permute-start.1 = (bf16[1024,128]{0,1:T(8,128)(2,1)S(1)}, bf16[1024,128]{0,1:T(8,128)(2,1)S(1)}, u32[]{:S(2)}, u32[]{:S(2)}) collective-permute-start(bf16[1024,128]{0,1:T(8,128)(2,1)S(1)} %bitcast.85), channel_id=1, source_target_pairs={{0,7},{1,0},{2,1},{3,2},{4,3},{5,4},{6,5},{7,6},{8,15},{9,8},{10,9... | collective-permute-start | bytes 786440 | tf_op jit(solution)/shard_map/ppermute | solution.py:201
  133.3 8.2 %collective-permute-done.1 = bf16[1024,128]{0,1:T(8,128)(2,1)S(1)} collective-permute-done((bf16[1024,128]{0,1:T(8,128)(2,1)S(1)}, bf16[1024,128]{0,1:T(8,128)(2,1)S(1)}, u32[]{:S(2)}, u32[]{:S(2)}) %collective-permute-start.1) | collective-permute-done | bytes 262176 | tf_op jit(solution)/shard_map/ppermute | solution.py:201
  141.5 3.7 %collective-permute-start.3 = (bf16[1024,128]{0,1:T(8,128)(2,1)S(1)}, bf16[1024,128]{0,1:T(8,128)(2,1)S(1)}, u32[]{:S(2)}, u32[]{:S(2)}) collective-permute-start(bf16[1024,128]{0,1:T(8,128)(2,1)S(1)} %collective-permute-done.1), channel_id=1, source_target_pairs={{0,7},{1,0},{2,1},{3,2},{4,3},{5,4},{6,5},{7,6},{8,15},{9,8},{10,9... | collective-permute-start | bytes 786440 | tf_op jit(solution)/shard_map/ppermute | solution.py:201
  145.2 1.6 broadcast_in_dim.42
  147.5 1.7 constant_dynamic-update-slice_fusion.6
  149.9 7.7 %collective-permute-done.3 = bf16[1024,128]{0,1:T(8,128)(2,1)S(1)} collective-permute-done((bf16[1024,128]{0,1:T(8,128)(2,1)S(1)}, bf16[1024,128]{0,1:T(8,128)(2,1)S(1)}, u32[]{:S(2)}, u32[]{:S(2)}) %collective-permute-start.3) | collective-permute-done | bytes 262176 | tf_op jit(solution)/shard_map/ppermute | solution.py:201
  157.6 3.7 %collective-permute-start.5 = (bf16[1024,128]{0,1:T(8,128)(2,1)S(1)}, bf16[1024,128]{0,1:T(8,128)(2,1)S(1)}, u32[]{:S(2)}, u32[]{:S(2)}) collective-permute-start(bf16[1024,128]{0,1:T(8,128)(2,1)S(1)} %collective-permute-done.3), channel_id=1, source_target_pairs={{0,7},{1,0},{2,1},{3,2},{4,3},{5,4},{6,5},{7,6},{8,15},{9,8},{10,9... | collective-permute-start | bytes 786440 | tf_op jit(solution)/shard_map/ppermute | solution.py:201
  162.8 2.6 %collective-permute-done.4 = bf16[1024,128]{0,1:T(8,128)(2,1)S(1)} collective-permute-done((bf16[1024,128]{0,1:T(8,128)(2,1)S(1)}, bf16[1024,128]{0,1:T(8,128)(2,1)S(1)}, u32[]{:S(2)}, u32[]{:S(2)}) %collective-permute-start.4) | collective-permute-done | bytes 262176 | tf_op jit(solution)/shard_map/ppermute | solution.py:196
  165.4 14.1 %all-reduce.3.cloned.1.call-done = bf16[4,1,8,24,2048]{4,3,2,0,1:T(8,128)(2,1)} async-done(((bf16[4,1,8,24,2048]{4,3,2,0,1:T(8,128)(2,1)}), bf16[4,1,8,24,2048]{4,3,2,0,1:T(8,128)(2,1)}) %all-reduce.3.cloned.1.call-update) | async-done | bytes 3145744
  179.5 2.4 %dynamic-slice_bitcast_fusion = bf16[4,1,1,24,2048]{4,3,2,1,0:T(8,128)(2,1)} fusion(bf16[4,1,8,24,2048]{4,3,2,0,1:T(8,128)(2,1)} %all-reduce.3.cloned.1.call-done, u32[]{:T(128)} %bitcast.27), kind=kLoop, calls=%fused_computation.76 | loop fusion | bytes 786436 | tf_op jit(solution)/shard_map/reduce_scatter | solution.py:250
  181.9 11.7 %all-to-all-start.1 = ((bf16[4,1,1,24,2048]{4,3,2,1,0:T(8,128)(2,1)}), bf16[4,1,1,24,2048]{4,3,2,1,0:T(8,128)(2,1)S(1)}, u32[]{:S(2)}, u32[]{:S(2)}) async-start(bf16[4,1,1,24,2048]{4,3,2,1,0:T(8,128)(2,1)} %dynamic-slice_bitcast_fusion), calls=%async_computation.1 | async-start | bytes 786432 | tf_op jit(solution)/shard_map/all_to_all | solution.py:265
  195.7 3.3 %convolution_convert_fusion.3 = bf16[1024,256]{1,0:T(8,128)(2,1)} fusion(bf16[1024,1024]{0,1:T(8,128)(2,1)} %constant_dynamic-update-slice_fusion, bf16[1024,256]{1,0:T(8,128)(2,1)} %param.29), kind=kOutput, calls=%fused_computation.60 | convolution fusion | flops 537133056 | bytes 3145728 | tf_op jit(solution)/shard_map/dot_general | solution.py:208
  201.4 16.2 %reduce-scatter.3.cloned.1.call-done = bf16[1,1,1,32,2048]{4,3,2,1,0:T(8,128)(2,1)} async-done(((bf16[1,1,8,32,2048]{4,3,2,1,0:T(8,128)(2,1)}), bf16[1,1,1,32,2048]{4,3,2,1,0:T(8,128)(2,1)}) %reduce-scatter.3.cloned.1.call-update) | async-done | bytes 131088 | tf_op jit(solution)/shard_map/reduce_scatter | solution.py:256
  217.6 1.6 fusion.62
  (106 shorter events, 15.9 us)
Async XLA Ops:
  8.0 71.7 %copy-start = (bf16[1,512,2048]{2,1,0:T(8,128)(2,1)S(1)}, bf16[1,512,2048]{2,1,0:T(8,128)(2,1)}, u32[]{:S(2)}) copy-start(bf16[1,512,2048]{2,1,0:T(8,128)(2,1)} %param.36) | copy-start | bytes 6291460
  8.0 7.8 %copy-start.3 = (bf16[256,2048]{1,0:T(8,128)(2,1)S(1)}, bf16[256,2048]{1,0:T(8,128)(2,1)}, u32[]{:S(2)}) copy-start(bf16[256,2048]{1,0:T(8,128)(2,1)} %param.30) | copy-start | bytes 3145732
  8.0 8.3 %copy-start.11 = (f32[2048]{0:T(1024)S(1)}, f32[2048]{0:T(1024)}, u32[]{:S(2)}) copy-start(f32[2048]{0:T(1024)} %param.31) | copy-start | bytes 24580
  9.0 9.0 %copy-start.5 = (s32[256,2]{1,0:T(8,128)}, s32[256,2]{1,0:T(8,128)S(1)}, u32[]{:S(2)}) copy-start(s32[256,2]{1,0:T(8,128)S(1)} %copy.32) | copy-start | bytes 6148
  26.1 6.7 %copy-start.12 = (f32[256]{0:T(256)S(1)}, f32[256]{0:T(256)}, u32[]{:S(2)}) copy-start(f32[256]{0:T(256)} %param.26) | copy-start | bytes 3076
  26.1 48.1 %all-to-all-start = ((bf16[4,1,8,24,2048]{4,3,2,1,0:T(8,128)(2,1)}), bf16[4,1,8,24,2048]{4,3,2,1,0:T(8,128)(2,1)}, u32[]{:S(2)}, u32[]{:S(2)}) async-start(bf16[4,1,8,24,2048]{4,3,2,1,0:T(8,128)(2,1)} %broadcast_select_fusion), calls=%async_computation | async-start | bytes 6291456 | tf_op jit(solution)/shard_map/all_to_all | solution.py:232
  31.4 3.5 %copy-start.9 = (bf16[1024,32]{0,1:T(8,128)(2,1)S(1)}, bf16[1024,32]{0,1:T(8,128)(2,1)}, u32[]{:S(2)}) copy-start(bf16[1024,32]{0,1:T(8,128)(2,1)} %param.24) | copy-start | bytes 196612
  31.4 5.1 %copy-start.14 = (bf16[512,192]{0,1:T(8,128)(2,1)S(1)}, bf16[512,192]{0,1:T(8,128)(2,1)}, u32[]{:S(2)}) copy-start(bf16[512,192]{0,1:T(8,128)(2,1)} %param.27) | copy-start | bytes 589828
  31.4 5.1 %copy-start.15 = (f32[512]{0:T(512)S(1)}, f32[512]{0:T(512)}, u32[]{:S(2)}) copy-start(f32[512]{0:T(512)} %param.25) | copy-start | bytes 6148
  31.4 70.1 %all-gather.2.cloned.1.call-start = ((), (), s32[]{:S(2)}) async-start(), calls=%async_computation.3 | async-start | bytes 2621440 | tf_op jit(solution)/shard_map/all_gather | solution.py:146
  34.9 144.6 %all-reduce.3.cloned.1.call-start = ((), (), s32[]{:S(2)}) async-start(), calls=%async_computation.5 | async-start | bytes 6291456
  38.3 0.9 copy-start.6
  87.9 129.7 %reduce-scatter.3.cloned.1.call-start = ((), (), s32[]{:S(2)}) async-start(), calls=%async_computation.4 | async-start | bytes 1179648 | tf_op jit(solution)/shard_map/reduce_scatter | solution.py:256
  88.0 12.3 %copy-start.4 = (bf16[2048,256]{1,0:T(8,128)(2,1)S(1)}, bf16[2048,256]{1,0:T(8,128)(2,1)}, u32[]{:S(2)}) copy-start(bf16[2048,256]{1,0:T(8,128)(2,1)} %param.37) | copy-start | bytes 3145732
  112.5 1.1 copy-start.7
  112.5 1.2 copy-start.1
  113.7 1.5 copy-start.8
  115.2 0.8 copy-start.2
  123.1 8.8 %copy-start.13 = (f32[256,2]{0,1:T(2,128)S(1)}, f32[256,2]{0,1:T(2,128)}, u32[]{:S(2)}) copy-start(f32[256,2]{0,1:T(2,128)} %param.33) | copy-start | bytes 6148
  123.1 9.6 %copy-start.16 = (u32[32]{0:T(128)S(1)}, u32[32]{0:T(128)}, u32[]{:S(2)}) copy-start(u32[32]{0:T(128)} %constant.155) | copy-start | bytes 388
  123.1 8.7 %collective-permute-start = (bf16[1024,128]{0,1:T(8,128)(2,1)S(1)}, bf16[1024,128]{0,1:T(8,128)(2,1)}, u32[]{:S(2)}, u32[]{:S(2)}) collective-permute-start(bf16[1024,128]{0,1:T(8,128)(2,1)S(1)} %bitcast.84), channel_id=1, source_target_pairs={{0,1},{1,2},{2,3},{3,4},{4,5},{5,6},{6,7},{7,0},{8,9},{9,10},{10,1... | collective-permute-start | bytes 786440 | tf_op jit(solution)/shard_map/ppermute | solution.py:196
  127.4 14.1 %collective-permute-start.1 = (bf16[1024,128]{0,1:T(8,128)(2,1)S(1)}, bf16[1024,128]{0,1:T(8,128)(2,1)S(1)}, u32[]{:S(2)}, u32[]{:S(2)}) collective-permute-start(bf16[1024,128]{0,1:T(8,128)(2,1)S(1)} %bitcast.85), channel_id=1, source_target_pairs={{0,7},{1,0},{2,1},{3,2},{4,3},{5,4},{6,5},{7,6},{8,15},{9,8},{10,9... | collective-permute-start | bytes 786440 | tf_op jit(solution)/shard_map/ppermute | solution.py:201
  131.8 17.4 %collective-permute-start.2 = (bf16[1024,128]{0,1:T(8,128)(2,1)}, bf16[1024,128]{0,1:T(8,128)(2,1)S(1)}, u32[]{:S(2)}, u32[]{:S(2)}) collective-permute-start(bf16[1024,128]{0,1:T(8,128)(2,1)} %collective-permute-done), channel_id=1, source_target_pairs={{0,1},{1,2},{2,3},{3,4},{4,5},{5,6},{6,7},{7,0},{8,9},{9,10},{10,1... | collective-permute-start | bytes 786440 | tf_op jit(solution)/shard_map/ppermute | solution.py:196
  141.5 16.1 %collective-permute-start.3 = (bf16[1024,128]{0,1:T(8,128)(2,1)S(1)}, bf16[1024,128]{0,1:T(8,128)(2,1)S(1)}, u32[]{:S(2)}, u32[]{:S(2)}) collective-permute-start(bf16[1024,128]{0,1:T(8,128)(2,1)S(1)} %collective-permute-done.1), channel_id=1, source_target_pairs={{0,7},{1,0},{2,1},{3,2},{4,3},{5,4},{6,5},{7,6},{8,15},{9,8},{10,9... | collective-permute-start | bytes 786440 | tf_op jit(solution)/shard_map/ppermute | solution.py:201
  149.2 16.1 %collective-permute-start.4 = (bf16[1024,128]{0,1:T(8,128)(2,1)S(1)}, bf16[1024,128]{0,1:T(8,128)(2,1)S(1)}, u32[]{:S(2)}, u32[]{:S(2)}) collective-permute-start(bf16[1024,128]{0,1:T(8,128)(2,1)S(1)} %collective-permute-done.2), channel_id=1, source_target_pairs={{0,1},{1,2},{2,3},{3,4},{4,5},{5,6},{6,7},{7,0},{8,9},{9,10},{10,1... | collective-permute-start | bytes 786440 | tf_op jit(solution)/shard_map/ppermute | solution.py:196
  157.6 36.7 %collective-permute-start.5 = (bf16[1024,128]{0,1:T(8,128)(2,1)S(1)}, bf16[1024,128]{0,1:T(8,128)(2,1)S(1)}, u32[]{:S(2)}, u32[]{:S(2)}) collective-permute-start(bf16[1024,128]{0,1:T(8,128)(2,1)S(1)} %collective-permute-done.3), channel_id=1, source_target_pairs={{0,7},{1,0},{2,1},{3,2},{4,3},{5,4},{6,5},{7,6},{8,15},{9,8},{10,9... | collective-permute-start | bytes 786440 | tf_op jit(solution)/shard_map/ppermute | solution.py:201
  165.4 29.6 %collective-permute-start.6 = (bf16[1024,128]{0,1:T(8,128)(2,1)S(1)}, bf16[1024,128]{0,1:T(8,128)(2,1)S(1)}, u32[]{:S(2)}, u32[]{:S(2)}) collective-permute-start(bf16[1024,128]{0,1:T(8,128)(2,1)S(1)} %collective-permute-done.4), channel_id=1, source_target_pairs={{0,1},{1,2},{2,3},{3,4},{4,5},{5,6},{6,7},{7,0},{8,9},{9,10},{10,1... | collective-permute-start | bytes 786440 | tf_op jit(solution)/shard_map/ppermute | solution.py:196
  181.9 17.6 %all-to-all-start.1 = ((bf16[4,1,1,24,2048]{4,3,2,1,0:T(8,128)(2,1)}), bf16[4,1,1,24,2048]{4,3,2,1,0:T(8,128)(2,1)S(1)}, u32[]{:S(2)}, u32[]{:S(2)}) async-start(bf16[4,1,1,24,2048]{4,3,2,1,0:T(8,128)(2,1)} %dynamic-slice_bitcast_fusion), calls=%async_computation.1 | async-start | bytes 786432 | tf_op jit(solution)/shard_map/all_to_all | solution.py:265
  199.5 1.1 copy-start.10
Sparse Core Ops, SparseCore 0:
  35.0 58.9 all-gather.1
Sparse Core Ops, SparseCore 1:
  88.0 91.4 all-reduce.2
  181.6 35.9 reduce-scatter.2
